TPU v7x, 32 devices: a whole 2x2x4 slice. The times are simulated.
32 devices in a mesh: sp: 8 (over z, core), tp: 4 (over y, x).
Axes of the slice: x: 2, y: 2, z: 4, core: 2. Of those that a mesh axis runs over, the one named last changes fastest.
Arguments:
- wide_queries: bfloat16 [512, 2560], P('sp', 'tp'), may hold values from -512 to 512
- narrow_queries: bfloat16 [512, 1536], P('sp', 'tp'), may hold values from -512 to 512
- kv_latent: bfloat16 [512, 512], P('sp'), may hold values from -6 to 6
- rope_key: bfloat16 [512, 32], P('sp'), may hold values from -4 to 4
- latent_gain: float32 [512], replicated, may hold values from 0.1 to 1.9
- wide_kv_weight: bfloat16 [512, 4096], P(None, 'tp'), may hold values from -0.25 to 0.25
- narrow_kv_weight: bfloat16 [512, 2048], P(None, 'tp'), may hold values from -0.25 to 0.25
- wide_out_weight: bfloat16 [2048, 2048], P('tp'), may hold values from -0.4375 to 0.4375
- narrow_out_weight: bfloat16 [1024, 2048], P('tp'), may hold values from -0.4375 to 0.4375
- residual: bfloat16 [512, 2048], P('sp'), may hold values from -6 to 6
- norm_gain: float32 [2048], replicated, may hold values from 0.1 to 1.9
- route_ids: int32 [512, 2], P('sp'), may hold values from 0 to 15, all different within a row; in each aligned block of 64 rows (0 to 63, 64 to 127, ...) at most 12 rows name the same one
- route_weights: float32 [512, 2], P('sp'), may hold values from 0.3 to 1.3
- expert_gate: bfloat16 [16, 2048, 1024], P('sp', None, 'tp'), may hold values from -0.125 to 0.125
- expert_up: bfloat16 [16, 2048, 1024], P('sp', None, 'tp'), may hold values from -0.125 to 0.125
- expert_down: bfloat16 [16, 1024, 2048], P('sp', 'tp'), may hold values from -0.1875 to 0.1875
- shared_gate: bfloat16 [2048, 1024], P(None, 'tp'), may hold values from -0.125 to 0.125
- shared_up: bfloat16 [2048, 1024], P(None, 'tp'), may hold values from -0.125 to 0.125
- shared_down: bfloat16 [1024, 2048], P('tp'), may hold values from -0.1875 to 0.1875
Outputs:
- mixed_out: bfloat16 [512, 2048], P('sp', 'tp')
Inputs may be any that keep to these rules, and one draw needn't show every extreme that they name: `route_ids`: in the rows of one index of sp (aligned blocks of 64 rows) no expert is named by more than 12 rows, and some expert by exactly that many; each row names 2 different experts.
All inputs are finite; a program needn't handle non-finite values.
Results may differ from a plain program's by a relative error of at most 0.018.
Values may be sent and summed in bfloat16 or wider, within the bound.
A program may use at most 64 MiB of HBM per device.

v0:
```python
import jax
import jax.numpy as jnp
from jax import lax
from jax.sharding import PartitionSpec as P

D_MODEL = 2048
WIDE_NOPE = 128
WIDE_VALUE = 128
NARROW_NOPE = 64
NARROW_VALUE = 64
ROPE_DIM = 32


THETA = 10000.0
EPS = 1e-06
FLOOR = -1e30


def rounded(values):
    return lax.optimization_barrier(values.astype(jnp.bfloat16)).astype(jnp.float32)


def rotate(values, positions):
    half_width = values.shape[-1] // 2
    frequency = THETA ** (-2.0 * jnp.arange(half_width, dtype=jnp.float32) / values.shape[-1])
    angles = positions.astype(jnp.float32)[:, None] * frequency[None, :]
    if values.ndim == 3:
        angles = angles[:, None, :]
    cosine = jnp.cos(angles)
    sine_part = jnp.sin(angles)
    as_float = values.astype(jnp.float32)
    first_half = as_float[..., :half_width]
    second_half = as_float[..., half_width:]
    return jnp.concatenate(
        [
            first_half * cosine - second_half * sine_part,
            second_half * cosine + first_half * sine_part,
        ],
        axis=-1,
    ).astype(jnp.bfloat16)


def rms_scale(values, gain):
    as_float = values.astype(jnp.float32)
    scaled = as_float * lax.rsqrt(jnp.mean(as_float * as_float, axis=-1, keepdims=True) + EPS)
    return (scaled * gain).astype(jnp.bfloat16)


def fresh_state(head_count, query_count, value_width):
    return (
        jnp.full((head_count, query_count), FLOOR, jnp.float32),
        jnp.zeros((head_count, query_count), jnp.float32),
        jnp.zeros((head_count, query_count, value_width), jnp.float32),
    )


def update(carry_part, queries, nope_width, kv_rows, rot_rows, query_pos, key_pos):
    row_peak, row_total, summed = carry_part
    head_count = queries.shape[1]
    key_value = kv_rows.reshape(kv_rows.shape[0], head_count, -1)
    values = key_value[..., nope_width:]
    shared_rot = jnp.broadcast_to(
        rot_rows[:, None, :], (rot_rows.shape[0], head_count, rot_rows.shape[1])
    )
    whole_keys = jnp.concatenate([key_value[..., :nope_width], shared_rot], axis=-1)
    scores = jnp.einsum("qhd,khd->hqk", queries, whole_keys, preferred_element_type=jnp.float32)
    scores = scores * queries.shape[-1] ** (-0.5)
    allowed = (query_pos[:, None] >= key_pos[None, :])[None]
    newest = jnp.maximum(row_peak, jnp.max(jnp.where(allowed, scores, FLOOR), axis=-1))
    weights = jnp.where(allowed, jnp.exp(scores - newest[..., None]), 0.0)
    row_total = jnp.sum(weights, axis=-1)
    summed = jnp.einsum(
        "hqk,khv->hqv", weights.astype(jnp.bfloat16), values, preferred_element_type=jnp.float32
    )
    return (newest, row_total, summed)


def local(
    wide_queries,
    narrow_queries,
    kv_latent,
    rope_key,
    latent_gain,
    wide_kv_weight,
    narrow_kv_weight,
    wide_out_weight,
    narrow_out_weight,
    residual,
    norm_gain,
    route_ids,
    route_weights,
    expert_gate,
    expert_up,
    expert_down,
    shared_gate,
    shared_up,
    shared_down,
):
    tok_rows = residual.shape[0]
    positions = lax.axis_index("sp") * tok_rows + jnp.arange(tok_rows, dtype=jnp.int32)
    wide_count = wide_out_weight.shape[0] // WIDE_VALUE
    narrow_count = narrow_out_weight.shape[0] // NARROW_VALUE
    wide_q = wide_queries.reshape(tok_rows, wide_count, WIDE_NOPE + ROPE_DIM)
    wide_q = jnp.concatenate(
        [wide_q[..., :WIDE_NOPE], rotate(wide_q[..., WIDE_NOPE:], positions)], axis=-1
    )
    narrow_q = narrow_queries.reshape(tok_rows, narrow_count, NARROW_NOPE + ROPE_DIM)
    narrow_q = jnp.concatenate(
        [narrow_q[..., :NARROW_NOPE], rotate(narrow_q[..., NARROW_NOPE:], positions)], axis=-1
    )
    key_rot = rotate(rope_key, positions)
    latent = rms_scale(kv_latent, latent_gain)
    initial = (
        fresh_state(wide_count, tok_rows, WIDE_VALUE),
        fresh_state(narrow_count, tok_rows, NARROW_VALUE),
    )
    pieces = (
        lax.all_gather(latent, "sp", axis=0, tiled=True),
        lax.all_gather(key_rot, "sp", axis=0, tiled=True),
    )
    wide_rows = jnp.dot(pieces[0], wide_kv_weight, preferred_element_type=jnp.float32).astype(
        jnp.bfloat16
    )
    narrow_rows = jnp.dot(pieces[0], narrow_kv_weight, preferred_element_type=jnp.float32).astype(
        jnp.bfloat16
    )
    rot_rows = pieces[1]
    key_pos = jnp.arange(rot_rows.shape[0], dtype=jnp.int32)
    final_state = (
        update(initial[0], wide_q, WIDE_NOPE, wide_rows, rot_rows, positions, key_pos),
        update(initial[1], narrow_q, NARROW_NOPE, narrow_rows, rot_rows, positions, key_pos),
    )
    wide_state, narrow_state = final_state
    wide_att = (wide_state[2] / wide_state[1][..., None]).astype(jnp.bfloat16)
    narrow_att = (narrow_state[2] / narrow_state[1][..., None]).astype(jnp.bfloat16)
    partial_proj = jnp.einsum(
        "hqv,hvd->qd",
        wide_att,
        wide_out_weight.reshape(wide_count, WIDE_VALUE, D_MODEL),
        preferred_element_type=jnp.float32,
    )
    partial_proj = partial_proj + jnp.einsum(
        "hqv,hvd->qd",
        narrow_att,
        narrow_out_weight.reshape(narrow_count, NARROW_VALUE, D_MODEL),
        preferred_element_type=jnp.float32,
    )
    proj_sum = lax.psum(rounded(partial_proj).astype(jnp.bfloat16), "tp").astype(jnp.float32)
    stream = (residual.astype(jnp.float32) + rounded(proj_sum)).astype(jnp.bfloat16)
    normed = rms_scale(stream, norm_gain)
    shared_hidden = (
        jax.nn.silu(jnp.dot(normed, shared_gate, preferred_element_type=jnp.float32))
        * jnp.dot(normed, shared_up, preferred_element_type=jnp.float32)
    ).astype(jnp.bfloat16)
    shared_part = jnp.dot(shared_hidden, shared_down, preferred_element_type=jnp.float32)
    shared_out = rounded(
        lax.psum_scatter(
            rounded(shared_part).astype(jnp.bfloat16), "tp", scatter_dimension=1, tiled=True
        ).astype(jnp.float32)
    )
    top_count = route_ids.shape[1]
    local_experts = expert_gate.shape[0]
    sp_count = lax.axis_size("sp")
    expert_total = sp_count * local_experts
    capacity = max(2, 3 * tok_rows * top_count // (2 * expert_total))
    flat_ids = route_ids.reshape(-1)
    one_hot = (flat_ids[:, None] == jnp.arange(expert_total, dtype=jnp.int32)[None, :]).astype(
        jnp.int32
    )
    earlier = jnp.cumsum(one_hot, axis=0) - one_hot
    slot_index = flat_ids * capacity + jnp.sum(earlier * one_hot, axis=1)
    copy_token = jnp.arange(tok_rows * top_count, dtype=jnp.int32) // top_count
    source_row = jnp.zeros((expert_total * capacity,), jnp.int32).at[slot_index].set(copy_token)
    filled = jnp.zeros((expert_total * capacity,), jnp.bfloat16).at[slot_index].set(1.0)
    column_width = D_MODEL // lax.axis_size("tp")
    column_start = lax.axis_index("tp") * column_width
    own_normed = lax.dynamic_slice_in_dim(normed, column_start, column_width, 1)
    outgoing = (own_normed[source_row] * filled[:, None]).reshape(
        sp_count, local_experts, capacity, column_width
    )
    arrived = lax.all_gather(
        lax.all_to_all(outgoing, "sp", split_axis=0, concat_axis=0, tiled=True),
        "tp",
        axis=3,
        tiled=True,
    )
    gate_value = jnp.einsum(
        "sejd,edf->sejf", arrived, expert_gate, preferred_element_type=jnp.float32
    )
    up_value = jnp.einsum("sejd,edf->sejf", arrived, expert_up, preferred_element_type=jnp.float32)
    hidden_units = (jax.nn.silu(gate_value) * up_value).astype(jnp.bfloat16)
    down_part = jnp.einsum(
        "sejf,efd->sejd", hidden_units, expert_down, preferred_element_type=jnp.float32
    )
    expert_result = lax.psum_scatter(
        rounded(down_part).astype(jnp.bfloat16), "tp", scatter_dimension=3, tiled=True
    )
    returned = lax.all_to_all(expert_result, "sp", split_axis=0, concat_axis=0, tiled=True)
    back_rows = returned.reshape(expert_total * capacity, column_width)[slot_index]
    routed = jnp.sum(
        back_rows.astype(jnp.float32).reshape(tok_rows, top_count, column_width)
        * route_weights[:, :, None],
        axis=1,
    )
    own_stream = lax.dynamic_slice_in_dim(stream, column_start, column_width, 1).astype(jnp.float32)
    return (own_stream + shared_out + routed).astype(jnp.bfloat16)


def solution(mesh):
    placed = (
        P("sp", "tp"),
        P("sp", "tp"),
        P("sp", None),
        P("sp", None),
        P(),
        P(None, "tp"),
        P(None, "tp"),
        P("tp", None),
        P("tp", None),
        P("sp", None),
        P(),
        P("sp", None),
        P("sp", None),
        P("sp", None, "tp"),
        P("sp", None, "tp"),
        P("sp", "tp", None),
        P(None, "tp"),
        P(None, "tp"),
        P("tp", None),
    )
    return jax.shard_map(
        local, mesh=mesh, in_specs=placed, out_specs=P("sp", "tp"), check_vma=False
    )
```

profile of v0, /device:TPU:0, one launch (start us, length us, event | category | flops | bytes accessed | tf_op | source)
XLA Modules:
  0.0 202.1 jit_solution(8818083878113061387)
XLA Ops:
  6.6 1.2 reshape.171
  7.9 0.7 convert_element_type.113
  8.6 0.1 multiply_cosine_fusion
  8.7 15.7 %all-gather = bf16[8,64,32]{1,2,0:T(8,128)(2,1)S(1)} all-gather(bf16[1,64,32]{1,2,0:T(8,128)(2,1)S(1)} %maximum_bitcast_fusion), channel_id=1, replica_groups=mesh['sp'=8,'tp'=4] {'sp'}, dimensions={0}, use_global_device_ids=true | all-gather | bytes 36864 | tf_op jit(solution)/shard_map/all_gather | solution.py:119
  24.4 0.1 reshape.213
  24.5 1.0 fusion.63
  25.5 0.9 fusion.65
  26.4 14.7 %all_gather.9 = bf16[512,512]{1,0:T(8,128)(2,1)S(1)} all-gather(bf16[64,512]{1,0:T(8,128)(2,1)S(1)} %fusion.65), channel_id=1, replica_groups=mesh['sp'=8,'tp'=4] {'sp'}, dimensions={0}, use_global_device_ids=true | all-gather | bytes 589824 | tf_op jit(solution)/shard_map/all_gather | solution.py:118
  41.2 0.8 copy-done.1
  42.0 2.9 %convolution_convert_fusion.2 = bf16[512,1024]{1,0:T(8,128)(2,1)} fusion(bf16[512,512]{1,0:T(8,128)(2,1)S(1)} %all_gather.9, bf16[512,1024]{1,0:T(8,128)(2,1)} %param.24), kind=kOutput, calls=%fused_computation.16 | convolution fusion | flops 537395200 | bytes 2621440 | tf_op jit(solution)/shard_map/dot_general | solution.py:121
  44.9 1.9 reshape.172
  46.8 1.4 fusion.100
  48.2 1.3 copy.61
  49.9 0.2 subtract_convert_fusion.1
  50.1 0.4 select_reduce_fusion.1
  50.5 1.7 convolution_convert_fusion.3
  52.3 0.4 fusion.33
  52.7 0.8 copy-done.8
  53.5 0.2 fusion.35
  53.7 2.8 %convolution_bitcast_fusion.1 = f32[64,2048]{1,0:T(8,128)} fusion(bf16[4,64,2048]{2,1,0:T(8,128)(2,1)} %bitcast.76, f32[4,64,512]{2,1,0:T(8,128)} %copy-done.8, bf16[512,4,128]{0,2,1:T(8,128)(2,1)S(1)} %bitcast.74, f32[4,64]{1,0:T(4,128)S(1)} %broadcast_maximum_fusion, pred[64,512]{1,0:T(8,128)(4,1)S(1)} %iota_compare_fusion, f32[4,64]{1,0:T(4,128)S(1)} %fusion.35), kind=kOutput, calls=%fused_computation.8 | convolution fusion | flops 84312064 | bytes 2396160 | tf_op jit(solution)/shard_map/hqv,hvd->qd/dot_general | solution.py:142
  56.5 2.6 %fusion.2 = bf16[64,2048]{1,0:T(8,128)(2,1)} fusion(f32[64,2048]{1,0:T(8,128)} %convolution_bitcast_fusion.1, bf16[4,128,2048]{2,1,0:T(8,128)(2,1)S(1)} %bitcast.72, bf16[512,4,128]{2,1,0:T(4,128)(2,1)S(1)} %copy-done.3, f32[4,64,512]{2,1,0:T(8,128)} %copy-done.7, f32[4,64]{1,0:T(4,128)S(1)} %broadcast_maximum_fusion.1, ...), kind=kOutput, calls=%fused_computation.9 | convolution fusion | flops 168493056 | bytes 3966976 | tf_op jit(solution)/shard_map/hqv,hvd->qd/dot_general | solution.py:136
  59.5 0.1 mul.247
  59.6 0.1 eq.15
  59.8 0.2 reduce_window_sum.11
  60.0 0.2 select_reduce_fusion.2
  60.2 1.0 scatter_custom_fusion
  61.2 1.3 scatter_custom_fusion.1
  62.7 41.1 %all-reduce.2.cloned.1.call-done = bf16[64,2048]{1,0:T(8,128)(2,1)} async-done(((bf16[64,2048]{1,0:T(8,128)(2,1)}), bf16[64,2048]{1,0:T(8,128)(2,1)}) %all-reduce.2.cloned.1.call-update) | async-done | bytes 262160 | tf_op jit(solution)/shard_map/psum | solution.py:148
  103.8 1.1 fusion.28
  104.9 0.7 copy-done.5
  105.6 0.1 fusion.30
  105.8 1.0 gather_fusion
  106.9 0.1 broadcast_multiply_fusion
  107.0 0.2 copy.51
  107.2 12.8 %all_to_all.10 = bf16[8,2,12,512]{3,1,2,0:T(2,128)(2,1)S(1)} all-to-all(bf16[8,2,12,512]{3,1,2,0:T(2,128)(2,1)S(1)} %copy.51), channel_id=1, replica_groups=mesh['sp'=8,'tp'=4] {'sp'}, dimensions={0} | all-to-all | bytes 393216 | tf_op jit(solution)/shard_map/all_to_all | solution.py:182
  120.1 13.1 %all_gather.11 = bf16[8,2,12,2048]{3,2,0,1:T(8,128)(2,1)S(1)} all-gather(bf16[8,2,12,512]{3,2,0,1:T(8,128)(2,1)S(1)} %copy.52), channel_id=1, replica_groups=mesh['sp'=8,'tp'=4] {'tp'}, dimensions={3}, use_global_device_ids=true | all-gather | bytes 983040 | tf_op jit(solution)/shard_map/all_gather | solution.py:181
  133.2 1.2 fusion.8
  134.4 4.2 %fusion = bf16[8,2,12,2048]{3,2,0,1:T(8,128)(2,1)} fusion(bf16[2,256,2048]{2,1,0:T(8,128)(2,1)} %param.34, bf16[8,2,12,2048]{3,2,0,1:T(8,128)(2,1)S(1)} %all_gather.11, bf16[2,2048,256]{2,1,0:T(8,128)(2,1)} %param.33, f32[8,2,12,256]{3,2,0,1:T(8,128)} %fusion.8), kind=kOutput, calls=%fused_computation.5 | convolution fusion | flops 403341312 | bytes 5963776 | tf_op jit(solution)/shard_map/sejf,efd->sejd/dot_general | solution.py:192
  138.6 1.6 fusion.101
  140.2 2.7 %convolution_convert_fusion.1 = bf16[64,2048]{1,0:T(8,128)(2,1)} fusion(bf16[256,2048]{1,0:T(8,128)(2,1)S(1)} %copy-done.6, bf16[64,2048]{1,0:T(8,128)(2,1)S(1)} %fusion.30, bf16[2048,256]{1,0:T(8,128)(2,1)} %param.36, f32[64,256]{1,0:T(8,128)S(1)} %fusion.101), kind=kOutput, calls=%fused_computation.10 | convolution fusion | flops 134447104 | bytes 2686976 | tf_op jit(solution)/shard_map/dot_general | solution.py:155
  143.0 22.4 %reduce-scatter.5.cloned.1.call-done = bf16[8,2,12,512]{3,2,0,1:T(8,128)(2,1)} async-done(((bf16[8,2,12,2048]{3,2,0,1:T(8,128)(2,1)}), bf16[8,2,12,512]{3,2,0,1:T(8,128)(2,1)}) %reduce-scatter.5.cloned.1.call-update) | async-done | bytes 196624 | tf_op jit(solution)/shard_map/reduce_scatter | solution.py:195
  165.4 1.8 copy.53
  167.2 4.6 %all-to-all-start.1 = ((bf16[8,2,12,512]{3,1,2,0:T(2,128)(2,1)}), bf16[8,2,12,512]{3,1,2,0:T(2,128)(2,1)S(1)}, u32[]{:S(2)}, u32[]{:S(2)}) async-start(bf16[8,2,12,512]{3,1,2,0:T(2,128)(2,1)} %copy.53), calls=%async_computation.3 | async-start | bytes 393216 | tf_op jit(solution)/shard_map/all_to_all | solution.py:198
  171.9 20.6 %reduce-scatter.3.cloned.1.call-done = bf16[64,512]{1,0:T(8,128)(2,1)} async-done(((bf16[64,2048]{1,0:T(8,128)(2,1)}), bf16[64,512]{1,0:T(8,128)(2,1)}) %reduce-scatter.3.cloned.1.call-update) | async-done | bytes 65552 | tf_op jit(solution)/shard_map/reduce_scatter | solution.py:157
  192.6 0.8 gather_fusion.1
  193.5 0.2 reshape.178
  193.7 0.4 multiply_reduce_fusion
  194.1 1.5 add_convert_fusion.1
  (76 shorter events, 1.5 us)
Async XLA Ops:
  6.5 50.0 %copy-start = (bf16[512,2048]{1,0:T(8,128)(2,1)S(1)}, bf16[512,2048]{1,0:T(8,128)(2,1)}, u32[]{:S(2)}) copy-start(bf16[512,2048]{1,0:T(8,128)(2,1)} %param.26) | copy-start | bytes 6291460
  6.5 97.2 %all-reduce.2.cloned.1.call-start = ((), (), s32[]{:S(2)}) async-start(), calls=%async_computation.4 | async-start | bytes 524288 | tf_op jit(solution)/shard_map/psum | solution.py:148
  7.7 37.2 %copy-start.9 = (bf16[64,4,160]{2,1,0:T(4,128)(2,1)}, bf16[64,4,160]{2,1,0:T(4,128)(2,1)S(1)}, u32[]{:S(2)}) copy-start(bf16[64,4,160]{2,1,0:T(4,128)(2,1)S(1)} %reshape.171) | copy-start | bytes 245764
  41.2 0.8 copy-start.1
  46.8 2.7 %copy-start.12 = (bf16[64,384]{1,0:T(8,128)(2,1)S(1)}, bf16[64,384]{1,0:T(8,128)(2,1)}, u32[]{:S(2)}) copy-start(bf16[64,384]{1,0:T(8,128)(2,1)} %param.20) | copy-start | bytes 147460
  46.8 3.1 %slice-start.1 = ((bf16[64,4,160]{2,1,0:T(4,128)(2,1)}), bf16[64,4,128]{2,1,0:T(4,128)(2,1)S(1)}, s32[]{:S(2)}) async-start(bf16[64,4,160]{2,1,0:T(4,128)(2,1)} %copy-done.9), calls=%async_computation.8 | async-start | bytes 131072 | tf_op jit(solution)/shard_map/slice | solution.py:105
  46.8 3.1 %slice-start = ((bf16[64,4,160]{2,1,0:T(4,128)(2,1)}), bf16[64,4,32]{2,1,0:T(4,128)(2,1)S(1)}, s32[]{:S(2)}) async-start(bf16[64,4,160]{2,1,0:T(4,128)(2,1)} %copy-done.9), calls=%async_computation.7 | async-start | bytes 131072 | tf_op jit(solution)/shard_map/slice | solution.py:105
  49.5 1.0 copy-start.2
  50.5 2.2 %copy-start.7 = (f32[4,64,512]{2,1,0:T(8,128)}, f32[4,64,512]{2,1,0:T(8,128)S(1)}, u32[]{:S(2)}) copy-start(f32[4,64,512]{2,1,0:T(8,128)S(1)} %get-tuple-element.24) | copy-start | bytes 1572868
  52.3 4.2 %copy-start.3 = (bf16[512,4,128]{2,1,0:T(4,128)(2,1)S(1)}, bf16[512,4,128]{2,1,0:T(4,128)(2,1)}, u32[]{:S(2)}) copy-start(bf16[512,4,128]{2,1,0:T(4,128)(2,1)} %get-tuple-element.9) | copy-start | bytes 1572868
  52.7 0.8 copy-start.8
  56.5 2.7 %copy-start.14 = (s32[64,2]{0,1:T(2,128)S(1)}, s32[64,2]{0,1:T(2,128)}, u32[]{:S(2)}) copy-start(s32[64,2]{0,1:T(2,128)} %param.30) | copy-start | bytes 1540
  56.5 47.2 %copy-start.10 = (bf16[64,2048]{1,0:T(8,128)(2,1)S(1)}, bf16[64,2048]{1,0:T(8,128)(2,1)}, u32[]{:S(2)}) copy-start(bf16[64,2048]{1,0:T(8,128)(2,1)} %param.28) | copy-start | bytes 786436
  56.5 49.1 %copy-start.13 = (f32[2048]{0:T(1024)S(1)}, f32[2048]{0:T(1024)}, u32[]{:S(2)}) copy-start(f32[2048]{0:T(1024)} %param.29) | copy-start | bytes 24580
  59.2 106.2 %reduce-scatter.5.cloned.1.call-start = ((), (), s32[]{:S(2)}) async-start(), calls=%async_computation.6 | async-start | bytes 1310720 | tf_op jit(solution)/shard_map/reduce_scatter | solution.py:195
  104.9 0.7 copy-start.5
  106.9 26.3 %copy-start.4 = (bf16[2,2048,256]{2,1,0:T(8,128)(2,1)S(1)}, bf16[2,2048,256]{2,1,0:T(8,128)(2,1)}, u32[]{:S(2)}) copy-start(bf16[2,2048,256]{2,1,0:T(8,128)(2,1)} %param.32) | copy-start | bytes 6291460
  138.5 1.7 copy-start.6
  138.5 54.0 %reduce-scatter.3.cloned.1.call-start = ((), (), s32[]{:S(2)}) async-start(), calls=%async_computation.5 | async-start | bytes 327680 | tf_op jit(solution)/shard_map/reduce_scatter | solution.py:157
  140.2 31.6 %copy-start.15 = (f32[64,2]{0,1:T(2,128)S(1)}, f32[64,2]{0,1:T(2,128)}, u32[]{:S(2)}) copy-start(f32[64,2]{0,1:T(2,128)} %param.31) | copy-start | bytes 1540
  167.2 25.3 %all-to-all-start.1 = ((bf16[8,2,12,512]{3,1,2,0:T(2,128)(2,1)}), bf16[8,2,12,512]{3,1,2,0:T(2,128)(2,1)S(1)}, u32[]{:S(2)}, u32[]{:S(2)}) async-start(bf16[8,2,12,512]{3,1,2,0:T(2,128)(2,1)} %copy.53), calls=%async_computation.3 | async-start | bytes 393216 | tf_op jit(solution)/shard_map/all_to_all | solution.py:198
  192.5 1.5 copy-start.11
Sparse Core Ops, SparseCore 0:
  59.3 44.4 all-reduce.1
  138.7 26.6 reduce-scatter.4
  168.1 24.3 reduce-scatter.2
where the time goes:
time: 203 us; the launch traced here: 202 us
  waiting for transfers between devices  84.1 us (41%)
  blocking collectives  56.4 us (28%)
  matrix products  20.4 us (10%)
  local copies, waits for them, and re-layouts  15.8 us (8%)
  between operations  13.6 us (7%)
  other arithmetic  6.96 us (3%)
  starting transfers between devices  4.71 us (2%)
    psum x1, waiting for transfers between devices, local(): lax.psum(rounded(partial_proj).astype(jnp.bfloat16), 'tp')  41.1 us
    reduce_scatter x1, waiting for transfers between devices, local(): lax.psum_scatter(rounded(down_part).astype(jnp.bfloat16), 'tp', scatter_d...  22.4 us
    reduce_scatter x1, waiting for transfers between devices, local(): lax.psum_scatter(rounded(shared_part).astype(jnp.bfloat16), 'tp', scatter...  20.6 us
    all_gather x1, blocking collectives, local(): lax.all_gather(key_rot, 'sp', axis=0, tiled=True)  15.7 us
    all_gather x1, blocking collectives, local(): lax.all_gather(latent, 'sp', axis=0, tiled=True)  14.7 us
    all_gather x1, blocking collectives, local(): lax.all_gather(lax.all_to_all(outgoing, 'sp', split_axis=0, concat_axis=0...  13.1 us
    all_to_all x1, blocking collectives, local(): lax.all_to_all(outgoing, 'sp', split_axis=0, concat_axis=0, tiled=True)  12.8 us
    all_to_all x1, starting transfers between devices, local(): lax.all_to_all(expert_result, 'sp', split_axis=0, concat_axis=0, tiled=True)  4.62 us
  transfers between devices with their start and end apart: 4, of which 3 were waited for; matrix products, arithmetic and copies ran while one was open for 5% of the time, Pallas kernels for 0%

commit v1 on v0

v1 whole, which is shorter than its diff:
```python
import functools
import math

import jax
import jax.numpy as jnp
from jax import lax
from jax.experimental import pallas as pl
from jax.experimental.pallas import tpu as pltpu
from jax.sharding import PartitionSpec as P

MESH = pl.DeviceIdType.MESH
WIDE_NOPE = 128
WIDE_VALUE = 128
NARROW_NOPE = 64
NARROW_VALUE = 64
ROPE_DIM = 32
LANES = 128

THETA = 10000.0
EPS = 1e-06
FLOOR = -1e30
F32 = jnp.float32
BF16 = jnp.bfloat16


def dot(a, b):
    return jnp.dot(a, b, preferred_element_type=F32)


def dot_t(a, b):
    return lax.dot_general(a, b, (((1,), (1,)), ((), ())), preferred_element_type=F32)


def one_hot(cond):
    return jnp.where(cond, 1.0, 0.0).astype(BF16)


def silu(v):
    return v / (1.0 + jnp.exp(-v))


def aligned_queries(queries, nope, heads, cosine, sine):
    rows, full = queries.shape[1], nope + ROPE_DIM

    def grid(width):
        shape = (rows, width)
        return lax.broadcasted_iota(jnp.int32, shape, 0), lax.broadcasted_iota(jnp.int32, shape, 1)

    i, j = grid(heads * LANES)
    d = j & (LANES - 1)
    plain = one_hot((i == (j >> 7) * full + d) & (d < nope))
    i, j = grid(LANES)
    start = (j >> 5) * full + nope
    d = j & (ROPE_DIM - 1)
    straight = one_hot(i == start + d)
    swapped = one_hot(i == start + (d ^ (ROPE_DIM // 2)))
    moved = dot(queries, plain).astype(BF16)
    turned = (dot(queries, straight) * cosine + dot(queries, swapped) * sine).astype(BF16)
    return moved, turned


def kernel(
    dims,
    wq_ref, nq_ref, kv_ref, rope_ref, lgain_ref, res_ref, ngain_ref, ids_ref, idst_ref, rw_ref,
    cos_ref, sin_ref, rowe_ref, rowc_ref, cole_ref, colc_ref,
    wkv_hbm, nkv_hbm, wout_hbm, nout_hbm, gate_hbm, up_hbm, down_hbm, sg_hbm, su_hbm, sd_hbm,
    out_ref,
    wkv, nkv, wout, nout, gate, up, down, sg, su, sd,
    blk, kv_all, part, part_in, strm, nrm, disp, arr, acc, shp, sh_in, pd, pd_in, ret, back,
    load_sem, ag_send, fw_send, ag_recv, p_send, p_recv, st_send, st_recv,
    di_send, rl_send, ar_recv, sh_send, sh_recv, pd_send, pd_recv, rt_send, rt_recv,
):
    S, T, R, cap = dims
    s, t = lax.axis_index("sp"), lax.axis_index("tp")
    core, z, nz = lax.rem(s, 2), s // 2, S // 2
    sib = s + 1 - 2 * core
    tok = kv_ref.shape[0]
    latent_dim = kv_ref.shape[1]
    CW = out_ref.shape[1]
    D = res_ref.shape[1]

    def rc(src, dst, ss, rs, sp, tp):
        return pltpu.make_async_remote_copy(
            src_ref=src, dst_ref=dst, send_sem=ss, recv_sem=rs, device_id=(sp, tp), device_id_type=MESH
        )

    def sp_at(d):
        return lax.rem(s + d, S)

    def tp_at(d):
        return lax.rem(t + d, T)

    def each(lo, hi, body):
        lax.fori_loop(lo, hi, lambda i, carry: (body(i), carry)[1], 0)

    loads = [
        pltpu.make_async_copy(src, dst, load_sem.at[i])
        for i, (src, dst) in enumerate(
            [
                (wkv_hbm, wkv), (nkv_hbm, nkv), (wout_hbm, wout), (nout_hbm, nout), (sg_hbm, sg),
                (su_hbm, su), (sd_hbm, sd), (gate_hbm, gate), (up_hbm, up), (down_hbm, down),
            ]
        )
    ]

    barrier = pltpu.get_barrier_semaphore()

    def greet_sp(d):
        pl.semaphore_signal(barrier, inc=1, device_id=(sp_at(d), t), device_id_type=MESH)

    def greet_tp(d):
        pl.semaphore_signal(barrier, inc=1, device_id=(s, tp_at(d)), device_id_type=MESH)

    each(1, S, greet_sp)
    each(1, T, greet_tp)
    for load in loads:
        load.start()

    cosine, sine = cos_ref[...], sin_ref[...]
    lat = kv_ref[...].astype(F32)
    lat = lat * lax.rsqrt(jnp.mean(lat * lat, axis=-1, keepdims=True) + EPS)
    blk[:, :latent_dim] = (lat * lgain_ref[...]).astype(BF16)
    i = lax.broadcasted_iota(jnp.int32, (ROPE_DIM, LANES), 0)
    j = lax.broadcasted_iota(jnp.int32, (ROPE_DIM, LANES), 1) & (ROPE_DIM - 1)
    rope = rope_ref[...]
    key_rot = dot(rope, one_hot(i == j)) * cosine + dot(rope, one_hot(i == (j ^ (ROPE_DIM // 2)))) * sine
    blk[:, latent_dim:] = key_rot.astype(BF16)
    pl.semaphore_wait(barrier, S - 1 + T - 1)

    def ag_copy(d):
        target = 2 * lax.rem(z + d, nz) + core
        return rc(blk, kv_all.at[s], ag_send.at[d], ag_recv.at[s], target, t)

    def fw_copy(d):
        b = 2 * lax.rem(z + d, nz) + core
        return rc(kv_all.at[b], kv_all.at[b], fw_send.at[d], ag_recv.at[b], sib, t)

    own_copy = rc(blk, kv_all.at[s], ag_send.at[0], ag_recv.at[s], sib, t)
    each(1, nz, lambda d: ag_copy(d).start())
    own_copy.start()
    kv_all[s] = blk[...]

    wide_heads = wq_ref.shape[1] // (WIDE_NOPE + ROPE_DIM)
    narrow_heads = nq_ref.shape[1] // (NARROW_NOPE + ROPE_DIM)
    wq, wr = aligned_queries(wq_ref[...], WIDE_NOPE, wide_heads, cosine, sine)
    nq, nr = aligned_queries(nq_ref[...], NARROW_NOPE, narrow_heads, cosine, sine)

    ii = lax.broadcasted_iota(jnp.int32, (tok, tok), 0)
    jj = lax.broadcasted_iota(jnp.int32, (tok, tok), 1)
    top = ids_ref.shape[1]
    hit_t = [ids_ref[:, k : k + 1] == rowe_ref[...] for k in range(top)]
    rank_t = dot(one_hot(jj < ii), one_hot(functools.reduce(jnp.logical_or, hit_t)))
    picks = [one_hot(h & (rank_t == rowc_ref[...])) for h in hit_t]
    hit = functools.reduce(jnp.logical_or, [cole_ref[...] == idst_ref[k : k + 1, :] for k in range(top)])
    spread = one_hot(hit & (dot(one_hot(hit), one_hot(ii < jj)) == colc_ref[...]))

    def relay_key(d):
        copy = fw_copy(nz - d)
        copy.wait_recv()
        copy.start()

    each(1, nz, relay_key)

    def rest_of_keys(d):
        b = 2 * lax.rem(z + d, nz) + 1 - core
        rc(blk, kv_all.at[b], ag_send.at[0], ag_recv.at[b], sib, t).wait_recv()

    each(0, nz, rest_of_keys)

    keys = S * tok
    latents = kv_all[:, :, :latent_dim].reshape(keys, latent_dim)
    kr = kv_all[:, :, latent_dim:].reshape(keys, LANES)
    query_pos = lax.broadcasted_iota(jnp.int32, (tok, keys), 0) + s * tok
    allowed = query_pos >= lax.broadcasted_iota(jnp.int32, (tok, keys), 1)
    lane = lax.broadcasted_iota(jnp.int32, (tok, LANES), 1)

    def attend(moved, turned, h, keys_h, values_h, width):
        rot = jnp.where((lane >> 5) == h, turned.astype(F32), 0.0).astype(BF16)
        query = jnp.concatenate([moved[:, h * LANES : (h + 1) * LANES], rot], axis=1)
        scores = dot_t(query, jnp.concatenate([keys_h, kr], axis=1)) * width ** (-0.5)
        scores = jnp.where(allowed, scores, FLOOR)
        weights = jnp.exp(scores - jnp.max(scores, axis=-1, keepdims=True))
        total = jnp.sum(weights, axis=-1, keepdims=True)
        return dot(weights.astype(BF16), values_h) / total

    loads[0].wait()
    attended = []
    for h in range(wide_heads):
        kv = dot(latents, wkv[:, h * 2 * LANES : (h + 1) * 2 * LANES]).astype(BF16)
        attended.append(
            attend(wq, wr, h, kv[:, :LANES], kv[:, LANES:], WIDE_NOPE + ROPE_DIM).astype(BF16)
        )
    loads[1].wait()
    narrow = []
    for h in range(narrow_heads):
        kv = dot(latents, nkv[:, h * LANES : (h + 1) * LANES]).astype(BF16)
        narrow.append(attend(nq, nr, h, kv, kv, NARROW_NOPE + ROPE_DIM))
    n_att = []
    for h in range(0, narrow_heads, 2):
        first = pltpu.roll(narrow[h], NARROW_VALUE, 1)
        if h + 1 < narrow_heads:
            n_att.append(jnp.where(lane < NARROW_VALUE, first, narrow[h + 1]).astype(BF16))
        else:
            n_att.append(first[:, :NARROW_VALUE].astype(BF16))
    w_att = jnp.concatenate(attended, axis=1) if wide_heads > 1 else attended[0]
    n_att = jnp.concatenate(n_att, axis=1) if len(n_att) > 1 else n_att[0]

    def columns(d):
        return pl.ds(pl.multiple_of(d * CW, CW), CW)

    loads[2].wait()
    loads[3].wait()

    def p_copy(d):
        tt = tp_at(d)
        return rc(part.at[tt], part_in.at[t], p_send.at[d], p_recv.at[t], s, tt)

    def project(d):
        tt = tp_at(d)
        part[tt] = (dot(w_att, wout[:, columns(tt)]) + dot(n_att, nout[:, columns(tt)])).astype(BF16)

    def project_and_send(d):
        project(d)
        p_copy(d).start()

    each(1, T, project_and_send)
    project(0)
    total = part[t].astype(F32)
    for d in range(1, T):
        tt = tp_at(d)
        rc(part.at[t], part_in.at[tt], p_send.at[d], p_recv.at[tt], s, tt).wait_recv()
        total = total + part_in[tt].astype(F32)
    strm[t] = (res_ref[:, columns(t)].astype(F32) + total.astype(BF16).astype(F32)).astype(BF16)

    def st_copy(d):
        return rc(strm.at[t], strm.at[t], st_send.at[d], st_recv.at[t], s, tp_at(d))

    each(1, T, lambda d: st_copy(d).start())
    own = strm[t].astype(F32)
    square = jnp.sum(own * own, axis=-1, keepdims=True)
    for d in range(1, T):
        tt = tp_at(d)
        rc(strm.at[t], strm.at[tt], st_send.at[d], st_recv.at[tt], s, tt).wait_recv()
        theirs = strm[tt].astype(F32)
        square = square + jnp.sum(theirs * theirs, axis=-1, keepdims=True)
    scale = lax.rsqrt(square / D + EPS)
    own_normed = (own * scale * ngain_ref[:, columns(t)]).astype(BF16)

    disp[...] = dot(spread, own_normed).reshape(S, R, CW).astype(BF16)

    def di_copy(d):
        to = lax.rem(s + S - d, S)
        return rc(disp.at[to], arr.at[t, s], di_send.at[d], ar_recv.at[t, s], to, t)

    def rl_own(d):
        return rc(disp.at[s], arr.at[t, s], rl_send.at[0, d], ar_recv.at[t, s], s, tp_at(d))

    each(1, S, lambda d: di_copy(d).start())
    each(1, T, lambda d: rl_own(d).start())
    arr[t, s] = disp[s]
    for tt in range(T):
        nrm[:, tt * CW : (tt + 1) * CW] = (
            strm[tt].astype(F32) * scale * ngain_ref[:, tt * CW : (tt + 1) * CW]
        ).astype(BF16)

    for i in range(4, 7):
        loads[i].wait()
    normed = nrm[...]
    hidden = (silu(dot(normed, sg[...])) * dot(normed, su[...])).astype(BF16)

    def sh_copy(d):
        tt = tp_at(d)
        return rc(shp.at[tt], sh_in.at[t], sh_send.at[d], sh_recv.at[t], s, tt)

    def shared_columns(d):
        tt = tp_at(d)
        shp[tt] = dot(hidden, sd[:, columns(tt)]).astype(BF16)

    def rl_copy(d, e):
        b = sp_at(d)
        return rc(arr.at[t, b], arr.at[t, b], rl_send.at[d, e], ar_recv.at[t, b], s, tp_at(e))

    def relay_rows(d):
        b = sp_at(d)
        rc(disp.at[s], arr.at[t, b], di_send.at[d], ar_recv.at[t, b], b, t).wait_recv()
        each(1, T, lambda e: rl_copy(d, e).start())

    each(1, S, relay_rows)

    def shared_and_send(d):
        shared_columns(d)
        sh_copy(d).start()

    each(1, T, shared_and_send)
    shared_columns(0)

    for i in range(7, 10):
        loads[i].wait()
    local_experts = gate.shape[0]
    acc[...] = jnp.zeros_like(acc)

    def expert_chunk(d):
        tt = tp_at(d)
        rows = arr[tt].astype(F32).reshape(S * R, CW).astype(BF16)
        for e in range(local_experts):
            acc[2 * e] += dot(rows, gate[e, columns(tt), :])
            acc[2 * e + 1] += dot(rows, up[e, columns(tt), :])

    def arrived_chunk(d):
        tt = tp_at(d)

        def arrived(b):
            rc(disp.at[s], arr.at[tt, b], rl_send.at[0, d], ar_recv.at[tt, b], s, tt).wait_recv()

        each(0, S, arrived)
        expert_chunk(d)

    expert_chunk(0)
    each(1, T, arrived_chunk)
    slot_expert = cole_ref[...]
    units = []
    for e in range(local_experts):
        value = silu(acc[2 * e]) * acc[2 * e + 1]
        mine = functools.reduce(
            jnp.logical_or, [slot_expert == b * local_experts + e for b in range(S)]
        )
        units.append(jnp.where(mine, value, 0.0).astype(BF16))

    def pd_copy(d, i):
        tt, b = tp_at(d), sp_at(i)
        return rc(pd.at[tt, b], pd_in.at[t, b], pd_send.at[d, i], pd_recv.at[t, b], s, tt)

    def down_columns(d):
        tt = tp_at(d)
        value = dot(units[0], down[0, :, columns(tt)])
        for e in range(1, local_experts):
            value = value + dot(units[e], down[e, :, columns(tt)])
        pd[tt] = value.reshape(S, R, CW).astype(BF16)

    def down_and_send(d):
        down_columns(d)
        each(1, S + 1, lambda i: pd_copy(d, lax.rem(i, S)).start())

    each(1, T, down_and_send)
    down_columns(0)

    shared = shp[t].astype(F32)
    for d in range(1, T):
        tt = tp_at(d)
        rc(shp.at[t], sh_in.at[tt], sh_send.at[d], sh_recv.at[tt], s, tt).wait_recv()
        shared = shared + sh_in[tt].astype(F32)
    base = strm[t].astype(F32) + shared.astype(BF16).astype(F32)

    def summed(b):
        value = pd[t, b].astype(F32)
        for d in range(1, T):
            tt = tp_at(d)
            rc(pd.at[t, b], pd_in.at[tt, b], pd_send.at[d, 0], pd_recv.at[tt, b], s, tt).wait_recv()
            value = value + pd_in[tt, b].astype(F32)
        return value.astype(BF16)

    def rt_copy(d):
        b = sp_at(d)
        return rc(ret.at[b], back.at[s], rt_send.at[d], rt_recv.at[s], b, t)

    def send_back(d):
        b = sp_at(d)
        ret[b] = summed(b)
        rt_copy(d).start()

    each(1, S, send_back)
    back[s] = summed(s)

    def returned(d):
        b = sp_at(d)
        rc(ret.at[s], back.at[b], rt_send.at[d], rt_recv.at[b], b, t).wait_recv()

    each(1, S, returned)
    rows = back[...].astype(F32).reshape(S * R, CW).astype(BF16)
    for k in range(top):
        base = base + dot(picks[k], rows) * rw_ref[:, k : k + 1]
    out_ref[...] = base.astype(BF16)

    own_copy.wait_send()
    each(1, nz, lambda d: ag_copy(d).wait_send())
    each(1, nz, lambda d: fw_copy(d).wait_send())
    each(1, S, lambda d: di_copy(d).wait_send())
    each(1, S, lambda d: rt_copy(d).wait_send())

    def close(e):
        p_copy(e).wait_send()
        st_copy(e).wait_send()
        sh_copy(e).wait_send()
        rl_own(e).wait_send()
        each(1, S, lambda d: rl_copy(d, e).wait_send())
        each(0, S, lambda i: pd_copy(e, i).wait_send())

    each(1, T, close)


def local(
    S, T,
    wide_queries, narrow_queries, kv_latent, rope_key, latent_gain, wide_kv_weight, narrow_kv_weight,
    wide_out_weight, narrow_out_weight, residual, norm_gain, route_ids, route_weights,
    expert_gate, expert_up, expert_down, shared_gate, shared_up, shared_down,
):
    tok, D = residual.shape
    latent_dim = kv_latent.shape[1]
    top = route_ids.shape[1]
    local_experts = expert_gate.shape[0]
    cap = max(2, 3 * tok * top // (2 * S * local_experts))
    R = -(-local_experts * cap // 8) * 8
    CW = D // T

    half = ROPE_DIM // 2
    positions = (lax.axis_index("sp") * tok + jnp.arange(tok, dtype=jnp.int32)).astype(F32)
    lane = jnp.arange(LANES, dtype=jnp.int32)
    frequency = THETA ** (-2.0 * (lane % half).astype(F32) / ROPE_DIM)
    angles = positions[:, None] * frequency[None, :]
    cosine = jnp.cos(angles)
    sine = jnp.where((lane % ROPE_DIM < half)[None, :], -1.0, 1.0) * jnp.sin(angles)

    slot = jnp.arange(S * R, dtype=jnp.int32)
    within = slot % R
    slot_expert = jnp.where(
        within < local_experts * cap, slot // R * local_experts + within // cap, -1
    ).astype(jnp.int32)
    slot_place = (within % cap).astype(F32)

    vm = pl.BlockSpec(memory_space=pltpu.VMEM)
    hbm = pl.BlockSpec(memory_space=pl.ANY)
    weights = (
        wide_kv_weight, narrow_kv_weight, wide_out_weight, narrow_out_weight,
        expert_gate, expert_up, expert_down, shared_gate, shared_up, shared_down,
    )
    small = (
        wide_queries, narrow_queries, kv_latent, rope_key, latent_gain[None, :], residual,
        norm_gain[None, :], route_ids, route_ids.T, route_weights, cosine, sine,
        slot_expert[None, :], slot_place[None, :], slot_expert[:, None], slot_place[:, None],
    )
    V = pltpu.VMEM
    sem = pltpu.SemaphoreType.DMA
    ff = expert_gate.shape[2]
    scratch = [V(w.shape, w.dtype) for w in weights] + [
        V((tok, latent_dim + LANES), BF16),
        V((S, tok, latent_dim + LANES), BF16),
        V((T, tok, CW), BF16),
        V((T, tok, CW), BF16),
        V((T, tok, CW), BF16),
        V((tok, D), BF16),
        V((S, R, CW), BF16),
        V((T, S, R, CW), BF16),
        V((2 * local_experts, S * R, ff), F32),
        V((T, tok, CW), BF16),
        V((T, tok, CW), BF16),
        V((T, S, R, CW), BF16),
        V((T, S, R, CW), BF16),
        V((S, R, CW), BF16),
        V((S, R, CW), BF16),
        sem((len(weights),)), sem((S // 2,)), sem((S // 2,)), sem((S,)),
        sem((T,)), sem((T,)), sem((T,)), sem((T,)),
        sem((S,)), sem((S, T)), sem((T, S)), sem((T,)), sem((T,)),
        sem((T, S)), sem((T, S)), sem((S,)), sem((S,)),
    ]
    return pl.pallas_call(
        functools.partial(kernel, (S, T, R, cap)),
        out_shape=jax.ShapeDtypeStruct((tok, CW), BF16),
        in_specs=[vm] * len(small) + [hbm] * len(weights),
        out_specs=vm,
        scratch_shapes=scratch,
        compiler_params=pltpu.CompilerParams(
            collective_id=0, has_side_effects=True, vmem_limit_bytes=60 * 1024 * 1024
        ),
    )(*small, *weights)


def solution(mesh):
    placed = (
        P("sp", "tp"),
        P("sp", "tp"),
        P("sp", None),
        P("sp", None),
        P(),
        P(None, "tp"),
        P(None, "tp"),
        P("tp", None),
        P("tp", None),
        P("sp", None),
        P(),
        P("sp", None),
        P("sp", None),
        P("sp", None, "tp"),
        P("sp", None, "tp"),
        P("sp", "tp", None),
        P(None, "tp"),
        P(None, "tp"),
        P("tp", None),
    )
    return jax.shard_map(
        functools.partial(local, mesh.shape["sp"], mesh.shape["tp"]),
        mesh=mesh, in_specs=placed, out_specs=P("sp", "tp"), check_vma=False,
    )
```

time: 203 us -> 70.7 us (0.35)
  waiting for transfers between devices: 84.1 us -> 0 us
  Pallas kernels: 0 us -> 62.5 us
  blocking collectives: 56.4 us -> 0 us
  matrix products: 20.4 us -> 0 us
  between operations: 13.6 us -> 0.01 us
  local copies, waits for them, and re-layouts: 15.8 us -> 5.61 us
  starting transfers between devices: 4.71 us -> 0 us
  other arithmetic: 6.96 us -> 2.27 us
    pallas_call x0 -> x1, Pallas kernels: none -> 62.5 us  [local(): pl.pallas_call(functools.partial(kernel, (S, T, R, cap)), out_shape=jax.S...]
    all_gather x3 -> x0, blocking collectives: 43.5 us -> none  [the longest x1 15.7 us: local(): lax.all_gather(key_rot, 'sp', axis=0, tiled=True)]
    reduce_scatter x2 -> x0, waiting for transfers between devices: 43 us -> none  [the longest x1 22.4 us: local(): lax.psum_scatter(rounded(down_part).astype(jnp.bfloat16), 'tp', scatter_d...]
    psum x1 -> x0, waiting for transfers between devices: 41.1 us -> none  [local(): lax.psum(rounded(partial_proj).astype(jnp.bfloat16), 'tp')]
    dot_general x10 -> x0, matrix products: 20.4 us -> none  [the longest x1 4.15 us: local(): jnp.einsum('sejf,efd->sejd', hidden_units, expert_down, preferred_element...]
    all_to_all x1 -> x0, blocking collectives: 12.8 us -> none  [local(): lax.all_to_all(outgoing, 'sp', split_axis=0, concat_axis=0, tiled=True)]
    all_to_all x1 -> x0, starting transfers between devices: 4.62 us -> none  [local(): lax.all_to_all(expert_result, 'sp', split_axis=0, concat_axis=0, tiled=True)]
    convert_element_type x7 -> x1, other arithmetic: 3.39 us -> 0.01 us  [local(): (lax.axis_index('sp') * tok + jnp.arange(tok, dtype=jnp.int32)).astype(F32)]
  transfers between devices with their start and end apart: 4 -> 0, of which waited for: 3 -> 0; matrix products, arithmetic and copies ran while one was open for 5% -> 0% of each run, Pallas kernels for 0% -> 0%
where the time goes in v1:
time: 70.7 us; the launch traced here: 70.4 us
  Pallas kernels  62.5 us (88%)
  local copies, waits for them, and re-layouts  5.61 us (8%)
  other arithmetic  2.27 us (3%)
    pallas_call x1, Pallas kernels, local(): pl.pallas_call(functools.partial(kernel, (S, T, R, cap)), out_shape=jax.S...  62.5 us
    unnamed x4, local copies, waits for them, and re-layouts  5.61 us
    select_n x2, other arithmetic, local(): jnp.where(within < local_experts * cap, slot // R * local_experts + withi...  1.44 us

profile of v1, /device:TPU:0, one launch (start us, length us, event | category | flops | bytes accessed | tf_op | source)
XLA Modules:
  0.0 70.4 jit_solution(1506497090449393223)
XLA Ops:
  0.0 0.6 compare_select_fusion
  0.6 1.4 %copy.20.rope_ref = bf16[64,32]{1,0:T(8,128)(2,1)} copy(bf16[64,32]{0,1:T(8,128)(2,1)} %param.22) | data formatting | bytes 8192 | tf_op args[3]
  2.0 1.4 %copy.22.rw_ref = f32[64,2]{1,0:T(8,128)} copy(f32[64,2]{0,1:T(2,128)} %param.31) | data formatting | bytes 1024 | tf_op args[12]
  3.4 1.4 %copy.21.ids_ref = s32[64,2]{1,0:T(8,128)} copy(s32[64,2]{0,1:T(2,128)} %param.30) | data formatting | bytes 1024 | tf_op args[11]
  4.8 0.8 %fusion.20 = (f32[64,128]{1,0:T(8,128)}, f32[64,128]{1,0:T(8,128)}) fusion(f32[128]{0:T(128)S(1)} %get-tuple-element.7, f32[128]{0:T(128)S(1)} %get-tuple-element.8, f32[64]{0:T(128)S(1)} %add_convert_fusion), kind=kLoop, calls=%fused_computation.28 | loop fusion | flops 16384 | bytes 66816 | tf_op jit(solution)/shard_map/mul | solution.py:421
  5.6 0.8 %fusion.8 = (s32[192,1]{1,0:T(8,128)}, f32[192,1]{1,0:T(8,128)}) fusion(), kind=kLoop, calls=%fused_computation.14 | loop fusion | flops 5568 | bytes 1536 | tf_op jit(solution)/shard_map/jit(_where)/select_n | solution.py:425
  6.4 62.5 %shard_map.181 = bf16[64,512]{1,0:T(8,128)(2,1)} custom-call(bf16[64,640]{1,0:T(8,128)(2,1)} %wq_ref.1, bf16[64,384]{1,0:T(8,128)(2,1)} %nq_ref.1, bf16[64,512]{1,0:T(8,128)(2,1)} %kv_ref.1, bf16[64,32]{1,0:T(8,128)(2,1)} %copy.20.rope_ref, f32[1,512]{1,0:T(1,128)} %bitcast.5, bf16[64,2048]{1,0:T(8,128)(2,1)} %res_ref.1, f32[1,2048]{1,0:T(1,128)} %bitcast.3, ...), custom_call_target="tpu_custom_call" | custom-call | tf_op jit(solution)/shard_map/pallas_call | solution.py:465
  69.0 1.5 %copy.24 = bf16[64,512]{1,0:T(8,128)(2,1)} copy(bf16[64,512]{1,0:T(8,128)(2,1)} %shard_map.181) | data formatting | bytes 131072
  (2 shorter events, 0.0 us)

commit v2 on v1

--- a/solution.py
+++ b/solution.py
@@ -61,12 +61,11 @@
 
 def kernel(
     dims,
-    wq_ref, nq_ref, kv_ref, rope_ref, lgain_ref, res_ref, ngain_ref, ids_ref, idst_ref, rw_ref,
-    cos_ref, sin_ref, rowe_ref, rowc_ref, cole_ref, colc_ref,
+    wq_ref, nq_ref, kv_ref, ropet_ref, lgain_ref, res_ref, ngain_ref, idst_ref, rwt_ref,
     wkv_hbm, nkv_hbm, wout_hbm, nout_hbm, gate_hbm, up_hbm, down_hbm, sg_hbm, su_hbm, sd_hbm,
     out_ref,
     wkv, nkv, wout, nout, gate, up, down, sg, su, sd,
-    blk, kv_all, part, part_in, strm, nrm, disp, arr, acc, shp, sh_in, pd, pd_in, ret, back,
+    blk, rot, kv_all, rot_all, part, part_in, strm, disp, arr, acc, shp, sh_in, pd, pd_in, ret, back,
     load_sem, ag_send, fw_send, ag_recv, p_send, p_recv, st_send, st_recv,
     di_send, rl_send, ar_recv, sh_send, sh_recv, pd_send, pd_recv, rt_send, rt_recv,
 ):
@@ -88,6 +87,8 @@
         return lax.rem(s + d, S)
 
     def tp_at(d):
+        if T == 4:
+            return 2 * lax.rem(t // 2 + (4 - d) // 2, 2) + lax.rem(t + d, 2)
         return lax.rem(t + d, T)
 
     def each(lo, hi, body):
@@ -116,67 +117,120 @@
     for load in loads:
         load.start()
 
-    cosine, sine = cos_ref[...], sin_ref[...]
+    half = ROPE_DIM // 2
+    lane = lax.broadcasted_iota(jnp.int32, (tok, LANES), 1)
+    row = lax.broadcasted_iota(jnp.int32, (tok, LANES), 0)
+    frequency = jnp.zeros((tok, LANES), F32)
+    for n in range(half):
+        frequency = jnp.where((lane & (half - 1)) == n, float(THETA ** (-2.0 * n / ROPE_DIM)), frequency)
+    angles = (s * tok + row).astype(F32) * frequency
+    cosine = jnp.cos(angles)
+    sine = jnp.where((lane & (ROPE_DIM - 1)) < half, -1.0, 1.0) * jnp.sin(angles)
     lat = kv_ref[...].astype(F32)
     lat = lat * lax.rsqrt(jnp.mean(lat * lat, axis=-1, keepdims=True) + EPS)
-    blk[:, :latent_dim] = (lat * lgain_ref[...]).astype(BF16)
+    blk[...] = (lat * lgain_ref[...]).astype(BF16)
     i = lax.broadcasted_iota(jnp.int32, (ROPE_DIM, LANES), 0)
     j = lax.broadcasted_iota(jnp.int32, (ROPE_DIM, LANES), 1) & (ROPE_DIM - 1)
-    rope = rope_ref[...]
+    ii = lax.broadcasted_iota(jnp.int32, (tok, tok), 0)
+    jj = lax.broadcasted_iota(jnp.int32, (tok, tok), 1)
+    eye = one_hot(ii == jj)
+    rope = dot_t(eye, ropet_ref[...]).astype(BF16)
     key_rot = dot(rope, one_hot(i == j)) * cosine + dot(rope, one_hot(i == (j ^ (ROPE_DIM // 2)))) * sine
-    blk[:, latent_dim:] = key_rot.astype(BF16)
+    group = tok * ROPE_DIM // LANES
+    lane_g = lax.broadcasted_iota(jnp.int32, (group, LANES), 1) // ROPE_DIM
+    packed = key_rot[:group]
+    for n in range(1, LANES // ROPE_DIM):
+        packed = jnp.where(lane_g == n, key_rot[n * group : (n + 1) * group], packed)
+    rot[...] = packed.astype(BF16)
     pl.semaphore_wait(barrier, S - 1 + T - 1)
 
-    def ag_copy(d):
+    def ag_copies(d):
         target = 2 * lax.rem(z + d, nz) + core
-        return rc(blk, kv_all.at[s], ag_send.at[d], ag_recv.at[s], target, t)
-
-    def fw_copy(d):
+        return (
+            rc(blk, kv_all.at[s], ag_send.at[d], ag_recv.at[s], target, t),
+            rc(rot, rot_all.at[s], ag_send.at[nz + d], ag_recv.at[S + s], target, t),
+        )
+
+    def fw_copies(d):
         b = 2 * lax.rem(z + d, nz) + core
-        return rc(kv_all.at[b], kv_all.at[b], fw_send.at[d], ag_recv.at[b], sib, t)
-
-    own_copy = rc(blk, kv_all.at[s], ag_send.at[0], ag_recv.at[s], sib, t)
-    each(1, nz, lambda d: ag_copy(d).start())
-    own_copy.start()
+        return (
+            rc(kv_all.at[b], kv_all.at[b], fw_send.at[d], ag_recv.at[b], sib, t),
+            rc(rot_all.at[b], rot_all.at[b], fw_send.at[nz + d], ag_recv.at[S + b], sib, t),
+        )
+
+    own_copies = (
+        rc(blk, kv_all.at[s], ag_send.at[0], ag_recv.at[s], sib, t),
+        rc(rot, rot_all.at[s], ag_send.at[nz], ag_recv.at[S + s], sib, t),
+    )
+
+    def start_keys(d):
+        for copy in ag_copies(d):
+            copy.start()
+
+    each(1, nz, start_keys)
+    for copy in own_copies:
+        copy.start()
     kv_all[s] = blk[...]
+    rot_all[s] = rot[...]
 
     wide_heads = wq_ref.shape[1] // (WIDE_NOPE + ROPE_DIM)
     narrow_heads = nq_ref.shape[1] // (NARROW_NOPE + ROPE_DIM)
     wq, wr = aligned_queries(wq_ref[...], WIDE_NOPE, wide_heads, cosine, sine)
     nq, nr = aligned_queries(nq_ref[...], NARROW_NOPE, narrow_heads, cosine, sine)
 
-    ii = lax.broadcasted_iota(jnp.int32, (tok, tok), 0)
-    jj = lax.broadcasted_iota(jnp.int32, (tok, tok), 1)
-    top = ids_ref.shape[1]
-    hit_t = [ids_ref[:, k : k + 1] == rowe_ref[...] for k in range(top)]
-    rank_t = dot(one_hot(jj < ii), one_hot(functools.reduce(jnp.logical_or, hit_t)))
-    picks = [one_hot(h & (rank_t == rowc_ref[...])) for h in hit_t]
-    hit = functools.reduce(jnp.logical_or, [cole_ref[...] == idst_ref[k : k + 1, :] for k in range(top)])
-    spread = one_hot(hit & (dot(one_hot(hit), one_hot(ii < jj)) == colc_ref[...]))
+    top = idst_ref.shape[0]
+    local_experts = gate.shape[0]
+
+    def slots(width):
+        slot = lax.broadcasted_iota(jnp.int32, (S * R, width), 0)
+        block = sum((slot >= b * R).astype(jnp.int32) for b in range(1, S))
+        within = slot - block * R
+        inner = sum(((within >= e * cap).astype(jnp.int32) for e in range(1, local_experts)), jnp.zeros_like(slot))
+        expert = jnp.where(within < local_experts * cap, block * local_experts + inner, -1)
+        return inner, expert, (within - inner * cap).astype(F32)
+
+    _, slot_expert, slot_place = slots(tok)
+    hits = [slot_expert == idst_ref[k : k + 1, :] for k in range(top)]
+    hit = functools.reduce(jnp.logical_or, hits)
+    placed = dot(one_hot(hit), one_hot(ii < jj)) == slot_place
+    spread = one_hot(hit & placed)
+    picks = [dot_t(eye, one_hot(h & placed)).astype(BF16) for h in hits]
+    own_weights = [
+        jnp.sum(jnp.where(ii == jj, rwt_ref[k : k + 1, :], 0.0), axis=1, keepdims=True) for k in range(top)
+    ]
 
     def relay_key(d):
-        copy = fw_copy(nz - d)
-        copy.wait_recv()
-        copy.start()
+        for copy in fw_copies(nz - d):
+            copy.wait_recv()
+            copy.start()
 
     each(1, nz, relay_key)
 
     def rest_of_keys(d):
         b = 2 * lax.rem(z + d, nz) + 1 - core
         rc(blk, kv_all.at[b], ag_send.at[0], ag_recv.at[b], sib, t).wait_recv()
+        rc(rot, rot_all.at[b], ag_send.at[nz], ag_recv.at[S + b], sib, t).wait_recv()
 
     each(0, nz, rest_of_keys)
 
     keys = S * tok
-    latents = kv_all[:, :, :latent_dim].reshape(keys, latent_dim)
-    kr = kv_all[:, :, latent_dim:].reshape(keys, LANES)
+    latents = kv_all[...].reshape(keys, latent_dim)
+    packed = rot_all[...].reshape(S * group, LANES)
+    i = lax.broadcasted_iota(jnp.int32, (LANES, LANES), 0)
+    j = lax.broadcasted_iota(jnp.int32, (LANES, LANES), 1) & (ROPE_DIM - 1)
+    kr = jnp.concatenate(
+        [
+            dot(packed, one_hot(i == n * ROPE_DIM + j)).astype(BF16).reshape(S, 1, group, LANES)
+            for n in range(LANES // ROPE_DIM)
+        ],
+        axis=1,
+    ).reshape(keys, LANES)
     query_pos = lax.broadcasted_iota(jnp.int32, (tok, keys), 0) + s * tok
     allowed = query_pos >= lax.broadcasted_iota(jnp.int32, (tok, keys), 1)
-    lane = lax.broadcasted_iota(jnp.int32, (tok, LANES), 1)
 
     def attend(moved, turned, h, keys_h, values_h, width):
-        rot = jnp.where((lane >> 5) == h, turned.astype(F32), 0.0).astype(BF16)
-        query = jnp.concatenate([moved[:, h * LANES : (h + 1) * LANES], rot], axis=1)
+        own_rot = jnp.where((lane >> 5) == h, turned.astype(F32), 0.0).astype(BF16)
+        query = jnp.concatenate([moved[:, h * LANES : (h + 1) * LANES], own_rot], axis=1)
         scores = dot_t(query, jnp.concatenate([keys_h, kr], axis=1)) * width ** (-0.5)
         scores = jnp.where(allowed, scores, FLOOR)
         weights = jnp.exp(scores - jnp.max(scores, axis=-1, keepdims=True))
@@ -215,16 +269,15 @@
         tt = tp_at(d)
         return rc(part.at[tt], part_in.at[t], p_send.at[d], p_recv.at[t], s, tt)
 
-    def project(d):
-        tt = tp_at(d)
+    def project_at(tt):
         part[tt] = (dot(w_att, wout[:, columns(tt)]) + dot(n_att, nout[:, columns(tt)])).astype(BF16)
 
     def project_and_send(d):
-        project(d)
+        project_at(tp_at(d))
         p_copy(d).start()
 
     each(1, T, project_and_send)
-    project(0)
+    project_at(t)
     total = part[t].astype(F32)
     for d in range(1, T):
         tt = tp_at(d)
@@ -258,22 +311,14 @@
     each(1, S, lambda d: di_copy(d).start())
     each(1, T, lambda d: rl_own(d).start())
     arr[t, s] = disp[s]
-    for tt in range(T):
-        nrm[:, tt * CW : (tt + 1) * CW] = (
-            strm[tt].astype(F32) * scale * ngain_ref[:, tt * CW : (tt + 1) * CW]
-        ).astype(BF16)
-
     for i in range(4, 7):
         loads[i].wait()
-    normed = nrm[...]
-    hidden = (silu(dot(normed, sg[...])) * dot(normed, su[...])).astype(BF16)
 
     def sh_copy(d):
         tt = tp_at(d)
         return rc(shp.at[tt], sh_in.at[t], sh_send.at[d], sh_recv.at[t], s, tt)
 
-    def shared_columns(d):
-        tt = tp_at(d)
+    def shared_columns(tt):
         shp[tt] = dot(hidden, sd[:, columns(tt)]).astype(BF16)
 
     def rl_copy(d, e):
@@ -285,22 +330,26 @@
         rc(disp.at[s], arr.at[t, b], di_send.at[d], ar_recv.at[t, b], b, t).wait_recv()
         each(1, T, lambda e: rl_copy(d, e).start())
 
-    each(1, S, relay_rows)
+    acc[...] = jnp.zeros_like(acc)
+    gated = jnp.zeros((tok, sg.shape[1]), F32)
+    upped = jnp.zeros((tok, sg.shape[1]), F32)
+    for n in range(T):
+        chunk = (strm[n].astype(F32) * scale * ngain_ref[:, n * CW : (n + 1) * CW]).astype(BF16)
+        gated += dot(chunk, sg[n * CW : (n + 1) * CW, :])
+        upped += dot(chunk, su[n * CW : (n + 1) * CW, :])
+        each(1 + (S - 1) * n // T, 1 + (S - 1) * (n + 1) // T, relay_rows)
+    hidden = (silu(gated) * upped).astype(BF16)
 
     def shared_and_send(d):
-        shared_columns(d)
+        shared_columns(tp_at(d))
         sh_copy(d).start()
 
     each(1, T, shared_and_send)
-    shared_columns(0)
+    shared_columns(t)
 
     for i in range(7, 10):
         loads[i].wait()
-    local_experts = gate.shape[0]
-    acc[...] = jnp.zeros_like(acc)
-
-    def expert_chunk(d):
-        tt = tp_at(d)
+    def expert_chunk(tt):
         rows = arr[tt].astype(F32).reshape(S * R, CW).astype(BF16)
         for e in range(local_experts):
             acc[2 * e] += dot(rows, gate[e, columns(tt), :])
@@ -313,36 +362,29 @@
             rc(disp.at[s], arr.at[tt, b], rl_send.at[0, d], ar_recv.at[tt, b], s, tt).wait_recv()
 
         each(0, S, arrived)
-        expert_chunk(d)
-
-    expert_chunk(0)
+        expert_chunk(tt)
+
+    expert_chunk(t)
     each(1, T, arrived_chunk)
-    slot_expert = cole_ref[...]
+    inner, _, _ = slots(gate.shape[2])
     units = []
     for e in range(local_experts):
         value = silu(acc[2 * e]) * acc[2 * e + 1]
-        mine = functools.reduce(
-            jnp.logical_or, [slot_expert == b * local_experts + e for b in range(S)]
-        )
-        units.append(jnp.where(mine, value, 0.0).astype(BF16))
+        units.append(jnp.where(inner == e, value, 0.0).astype(BF16))
 
     def pd_copy(d, i):
         tt, b = tp_at(d), sp_at(i)
         return rc(pd.at[tt, b], pd_in.at[t, b], pd_send.at[d, i], pd_recv.at[t, b], s, tt)
 
-    def down_columns(d):
-        tt = tp_at(d)
+    def down_columns(tt):
         value = dot(units[0], down[0, :, columns(tt)])
         for e in range(1, local_experts):
             value = value + dot(units[e], down[e, :, columns(tt)])
         pd[tt] = value.reshape(S, R, CW).astype(BF16)
 
-    def down_and_send(d):
-        down_columns(d)
-        each(1, S + 1, lambda i: pd_copy(d, lax.rem(i, S)).start())
-
-    each(1, T, down_and_send)
-    down_columns(0)
+    each(1, T, lambda d: down_columns(tp_at(d)))
+    each(1, S + 1, lambda i: each(1, T, lambda d: pd_copy(d, lax.rem(i, S)).start()))
+    down_columns(t)
 
     shared = shp[t].astype(F32)
     for d in range(1, T):
@@ -378,12 +420,16 @@
     each(1, S, returned)
     rows = back[...].astype(F32).reshape(S * R, CW).astype(BF16)
     for k in range(top):
-        base = base + dot(picks[k], rows) * rw_ref[:, k : k + 1]
+        base = base + dot(picks[k], rows) * own_weights[k]
     out_ref[...] = base.astype(BF16)
 
-    own_copy.wait_send()
-    each(1, nz, lambda d: ag_copy(d).wait_send())
-    each(1, nz, lambda d: fw_copy(d).wait_send())
+    def close_keys(d):
+        for copy in ag_copies(d) + fw_copies(d):
+            copy.wait_send()
+
+    for copy in own_copies:
+        copy.wait_send()
+    each(1, nz, close_keys)
     each(1, S, lambda d: di_copy(d).wait_send())
     each(1, S, lambda d: rt_copy(d).wait_send())
 
@@ -412,21 +458,6 @@
     R = -(-local_experts * cap // 8) * 8
     CW = D // T
 
-    half = ROPE_DIM // 2
-    positions = (lax.axis_index("sp") * tok + jnp.arange(tok, dtype=jnp.int32)).astype(F32)
-    lane = jnp.arange(LANES, dtype=jnp.int32)
-    frequency = THETA ** (-2.0 * (lane % half).astype(F32) / ROPE_DIM)
-    angles = positions[:, None] * frequency[None, :]
-    cosine = jnp.cos(angles)
-    sine = jnp.where((lane % ROPE_DIM < half)[None, :], -1.0, 1.0) * jnp.sin(angles)
-
-    slot = jnp.arange(S * R, dtype=jnp.int32)
-    within = slot % R
-    slot_expert = jnp.where(
-        within < local_experts * cap, slot // R * local_experts + within // cap, -1
-    ).astype(jnp.int32)
-    slot_place = (within % cap).astype(F32)
-
     vm = pl.BlockSpec(memory_space=pltpu.VMEM)
     hbm = pl.BlockSpec(memory_space=pl.ANY)
     weights = (
@@ -434,20 +465,20 @@
         expert_gate, expert_up, expert_down, shared_gate, shared_up, shared_down,
     )
     small = (
-        wide_queries, narrow_queries, kv_latent, rope_key, latent_gain[None, :], residual,
-        norm_gain[None, :], route_ids, route_ids.T, route_weights, cosine, sine,
-        slot_expert[None, :], slot_place[None, :], slot_expert[:, None], slot_place[:, None],
+        wide_queries, narrow_queries, kv_latent, rope_key.T, latent_gain[None, :], residual,
+        norm_gain[None, :], route_ids.T, route_weights.T,
     )
     V = pltpu.VMEM
     sem = pltpu.SemaphoreType.DMA
     ff = expert_gate.shape[2]
     scratch = [V(w.shape, w.dtype) for w in weights] + [
-        V((tok, latent_dim + LANES), BF16),
-        V((S, tok, latent_dim + LANES), BF16),
+        V((tok, latent_dim), BF16),
+        V((tok * ROPE_DIM // LANES, LANES), BF16),
+        V((S, tok, latent_dim), BF16),
+        V((S, tok * ROPE_DIM // LANES, LANES), BF16),
         V((T, tok, CW), BF16),
         V((T, tok, CW), BF16),
         V((T, tok, CW), BF16),
-        V((tok, D), BF16),
         V((S, R, CW), BF16),
         V((T, S, R, CW), BF16),
         V((2 * local_experts, S * R, ff), F32),
@@ -457,7 +488,7 @@
         V((T, S, R, CW), BF16),
         V((S, R, CW), BF16),
         V((S, R, CW), BF16),
-        sem((len(weights),)), sem((S // 2,)), sem((S // 2,)), sem((S,)),
+        sem((len(weights),)), sem((S,)), sem((S,)), sem((2 * S,)),
         sem((T,)), sem((T,)), sem((T,)), sem((T,)),
         sem((S,)), sem((S, T)), sem((T, S)), sem((T,)), sem((T,)),
         sem((T, S)), sem((T, S)), sem((S,)), sem((S,)),

time: 70.7 us -> 61.2 us (0.87)
  local copies, waits for them, and re-layouts: 5.61 us -> 1.47 us
  Pallas kernels: 62.5 us -> 59.5 us
  other arithmetic: 2.27 us -> 0 us
    unnamed x4 -> x1, local copies, waits for them, and re-layouts: 5.61 us -> 1.47 us
    pallas_call x1, Pallas kernels: 62.5 us -> 59.5 us  [local(): pl.pallas_call(functools.partial(kernel, (S, T, R, cap)), out_shape=jax.S...]
    select_n x3 -> x0, other arithmetic: 1.44 us -> none  [the longest x2 1.44 us: local(): jnp.where(within < local_experts * cap, slot // R * local_experts + withi...]
    mul x1 -> x0, other arithmetic: 0.82 us -> none  [local(): jnp.where((lane % ROPE_DIM < half)[None, :], -1.0, 1.0) * jnp.sin(angles)]
where the time goes in v2:
time: 61.2 us; the launch traced here: 61 us
  Pallas kernels  59.5 us (97%)
  local copies, waits for them, and re-layouts  1.47 us (2%)
    pallas_call x1, Pallas kernels, local(): pl.pallas_call(functools.partial(kernel, (S, T, R, cap)), out_shape=jax.S...  59.5 us
    unnamed x1, local copies, waits for them, and re-layouts  1.47 us

profile of v2, /device:TPU:0, one launch (start us, length us, event | category | flops | bytes accessed | tf_op | source)
XLA Modules:
  0.0 61.0 jit_solution(18051806842084012215)
XLA Ops:
  0.0 59.5 %shard_map.181 = bf16[64,512]{1,0:T(8,128)(2,1)} custom-call(bf16[64,640]{1,0:T(8,128)(2,1)} %wq_ref.1, bf16[64,384]{1,0:T(8,128)(2,1)} %nq_ref.1, bf16[64,512]{1,0:T(8,128)(2,1)} %kv_ref.1, bf16[32,64]{1,0:T(8,128)(2,1)} %bitcast.5, f32[1,512]{1,0:T(1,128)} %bitcast.7, bf16[64,2048]{1,0:T(8,128)(2,1)} %res_ref.1, f32[1,2048]{1,0:T(1,128)} %bitcast.6, ...), custom_call_target="tpu_custom_call" | custom-call | tf_op jit(solution)/shard_map/pallas_call | solution.py:496
  59.5 1.5 %copy.21 = bf16[64,512]{1,0:T(8,128)(2,1)} copy(bf16[64,512]{1,0:T(8,128)(2,1)} %shard_map.181) | data formatting | bytes 131072
